TPU v7x, 32 devices: a whole 2x2x4 slice. The times are simulated.
32 devices in a mesh: sp: 16 (over z, y, x), tp: 2 (over core).
Axes of the slice: x: 2, y: 2, z: 4, core: 2. Of those that a mesh axis runs over, the one named last changes fastest.
Arguments:
- prompt: bfloat16 [16, 1024, 2048], P('sp', None, 'tp'), may hold values from -6 to 6
- new_input: bfloat16 [16, 2048], P('sp', 'tp'), may hold values from -140 to 140
- w_query: bfloat16 [2048, 2048], P('sp', 'tp'), may hold values from -0.21875 to 0.21875
- w_key: bfloat16 [2048, 2048], P('sp', 'tp'), may hold values from -0.125 to 0.125
- w_value: bfloat16 [2048, 2048], P('sp', 'tp'), may hold values from -0.125 to 0.125
- lam: float32 [16], P('tp'), may hold values from 0.3 to 0.8
- out_gain: float32 [128], replicated, may hold values from 0.1 to 1.9
Outputs:
- key_cache: bfloat16 [16, 1024, 2048], P('sp', None, 'tp')
- value_cache: bfloat16 [16, 1024, 2048], P('sp', None, 'tp')
- first_read: bfloat16 [16, 16, 128], P('sp', 'tp')
All inputs are finite; a program needn't handle non-finite values.
Results may differ from a plain program's by a relative error of at most 0.02.
The roundings to bfloat16 on the way count: a program that leaves them out, or rounds other values in their place, can miss the bound.
Values may be sent and summed in bfloat16 or wider, within the bound.
A program may use at most 64 MiB of HBM per device.

v0:
```python
import jax
import jax.numpy as jnp
from jax import lax
from jax.sharding import PartitionSpec as P

MAP_DIM = 64
VAL_DIM = 128
LEN = 1024
rope_base = 500000.0
norm_eps = 1e-05


def rotate(vectors, angle):
    half = vectors.shape[-1] // 2
    cosine_table = jnp.cos(angle)
    sine = jnp.sin(angle)
    first = vectors[..., :half]
    second = vectors[..., half:]
    return jnp.concatenate(
        [first * cosine_table - second * sine, second * cosine_table + first * sine], axis=-1
    )


def inverse_freq():
    return rope_base ** (-(jnp.arange(MAP_DIM // 2, dtype=jnp.float32) * 2.0 / MAP_DIM))


def finish(mixed, lam, out_gain):
    diff = mixed[:, :, 0] - lam[None, :, None] * mixed[:, :, 1]
    normed = diff * lax.rsqrt(jnp.mean(diff * diff, axis=-1, keepdims=True) + norm_eps)
    return (normed * out_gain).astype(jnp.bfloat16)


def read_whole(query, keys, values, lam, out_gain):
    seqs, length, _ = keys.shape
    heads = lam.shape[0]
    key_maps = keys.reshape(seqs, length, heads, 2, MAP_DIM)
    value_heads = values.reshape(seqs, length, heads, VAL_DIM)
    attention_scores = jnp.einsum(
        "shmd,slhmd->shml", query, key_maps, preferred_element_type=jnp.float32
    ) * MAP_DIM ** (-0.5)
    weights = jax.nn.softmax(attention_scores, axis=-1)
    mixed = jnp.einsum(
        "shml,slhe->shme", weights, value_heads.astype(jnp.float32), precision=lax.Precision.HIGHEST
    )
    return finish(mixed, lam, out_gain)


def body(prompt, new_input, w_query, w_key, w_value, lam, out_gain):
    heads = lam.shape[0]
    seqs, count, _ = prompt.shape
    local_seqs = new_input.shape[0]
    inverse = inverse_freq()
    full_query, full_key, full_value = (
        lax.all_gather(w_query, "sp", axis=0, tiled=True),
        lax.all_gather(w_key, "sp", axis=0, tiled=True),
        lax.all_gather(w_value, "sp", axis=0, tiled=True),
    )
    pieces = (
        lax.all_gather(prompt, "tp", axis=2, tiled=True),
        lax.all_gather(new_input[:, None, :], "tp", axis=2, tiled=True),
    )
    width_piece = pieces[0].shape[2]
    row_piece = pieces[0].reshape(seqs * count, width_piece)
    fresh_piece = pieces[1][:, 0, :]
    key_sum = jnp.dot(row_piece, full_key, preferred_element_type=jnp.float32)
    weighted_value_sum = jnp.dot(row_piece, full_value, preferred_element_type=jnp.float32)
    query_sum = jnp.dot(fresh_piece, full_query, preferred_element_type=jnp.float32)
    positions = jnp.arange(count, dtype=jnp.float32)
    key_maps = rotate(
        key_sum.reshape(seqs, count, heads, 2, MAP_DIM), positions[:, None, None, None] * inverse
    )
    keys = key_maps.astype(jnp.bfloat16).reshape(seqs, count, heads * 2 * MAP_DIM)
    values = weighted_value_sum.astype(jnp.bfloat16).reshape(seqs, count, heads * VAL_DIM)
    query = rotate(
        query_sum.reshape(local_seqs, heads, 2, MAP_DIM), jnp.float32(LEN) * inverse
    ).astype(jnp.bfloat16)
    first_read = read_whole(query, keys, values, lam, out_gain)
    return (keys, values, first_read)


def solution(mesh):
    in_specs = (
        P("sp", None, "tp"),
        P("sp", "tp"),
        P("sp", "tp"),
        P("sp", "tp"),
        P("sp", "tp"),
        P("tp"),
        P(),
    )
    out_specs = (P("sp", None, "tp"), P("sp", None, "tp"), P("sp", "tp", None))
    return jax.shard_map(body, mesh=mesh, in_specs=in_specs, out_specs=out_specs, check_vma=False)
```

profile of v0, /device:TPU:0, one launch (start us, length us, event | category | flops | bytes accessed | tf_op | source)
XLA Modules:
  0.0 297.6 jit_solution(11442602501516390730)
XLA Ops:
  7.2 0.0 all-gather.8.cloned.1.call-start
  7.2 0.7 all-gather.8.cloned.1.call-update
  7.9 0.0 all-gather.12.cloned.1.call-start
  7.9 1.8 copy.16
  9.8 0.0 all-gather.6.cloned.1.call-start
  9.8 0.7 all-gather.6.cloned.1.call-update
  10.5 0.0 all-gather.10.cloned.1.call-start
  10.5 0.5 all-gather.10.cloned.1.call-update
  11.1 2.1 all-gather
  13.2 0.1 multiply_sine_fusion
  13.2 0.5 fusion.15
  13.8 75.3 %all-gather.8.cloned.1.call-done = bf16[2048,1024]{1,0:T(8,128)(2,1)} async-done(((bf16[128,1024]{1,0:T(8,128)(2,1)}), bf16[2048,1024]{1,0:T(8,128)(2,1)}) %all-gather.8.cloned.1.call-update) | async-done | bytes 4194320 | tf_op jit(solution)/shard_map/all_gather | solution.py:56
  89.1 6.5 %copy.15 = bf16[1024,2048]{1,0:T(8,128)(2,1)} copy(bf16[1024,2048]{0,1:T(8,128)(2,1)} %bitcast.59) | data formatting | bytes 8388608 | tf_op jit(solution)/shard_map/dot_general | solution.py:66
  95.6 84.1 %all-gather.12.cloned.1.call-done = bf16[2048,1024]{0,1:T(8,128)(2,1)} async-done(((bf16[128,1024]{0,1:T(8,128)(2,1)}), bf16[2048,1024]{0,1:T(8,128)(2,1)}) %all-gather.12.cloned.1.call-update) | async-done | bytes 4194320 | tf_op jit(solution)/shard_map/all_gather | solution.py:55
  179.7 3.9 %fusion.20 = f32[1,8,2,64]{3,0,2,1:T(1,128)S(1)} fusion(bf16[8,2,64,2048]{3,2,1,0:T(8,128)(2,1)} %bitcast.60, bf16[1,2048]{1,0:T(2,128)(2,1)S(1)} %all-gather), kind=kOutput, calls=%fused_computation.23 | convolution fusion | flops 4194304 | bytes 4202496 | tf_op jit(solution)/shard_map/dot_general | solution.py:68
  183.6 0.1 fusion.23
  183.7 0.1 maximum_bitcast_fusion
  183.8 9.3 %all-gather.6.cloned.1.call-done = bf16[1,1024,2048]{2,1,0:T(8,128)(2,1)} async-done(((bf16[1,1024,1024]{2,1,0:T(8,128)(2,1)}), bf16[1,1024,2048]{2,1,0:T(8,128)(2,1)}) %all-gather.6.cloned.1.call-update) | async-done | bytes 4194320 | tf_op jit(solution)/shard_map/all_gather | solution.py:60
  193.1 7.6 %fusion.4 = f32[1,1024,8,2,64]{1,4,3,2,0:T(8,128)S(1)} fusion(bf16[8,2,64,2048]{3,2,1,0:T(8,128)(2,1)} %bitcast.61, bf16[1,1024,2048]{2,1,0:T(8,128)(2,1)} %all-gather.6.cloned.1.call-done), kind=kOutput, calls=%fused_computation.4 | convolution fusion | flops 4294967296 | bytes 12582912 | tf_op jit(solution)/shard_map/dot_general | solution.py:66
  200.7 0.7 subtract_convert_fusion
  201.5 0.4 fusion.7
  201.9 0.1 fusion.25
  202.0 0.2 fusion.17
  202.2 0.2 pad_maximum_fusion
  202.4 70.2 %all-gather.10.cloned.1.call-done = bf16[2048,1024]{1,0:T(8,128)(2,1)} async-done(((bf16[128,1024]{1,0:T(8,128)(2,1)}), bf16[2048,1024]{1,0:T(8,128)(2,1)}) %all-gather.10.cloned.1.call-update) | async-done | bytes 4194320 | tf_op jit(solution)/shard_map/all_gather | solution.py:57
  272.6 8.0 %fusion.11 = bf16[1024,1024]{0,1:T(8,128)(2,1)S(1)} fusion(bf16[2048,1024]{1,0:T(8,128)(2,1)} %all-gather.10.cloned.1.call-done, bf16[1,1024,2048]{2,1,0:T(8,128)(2,1)} %all-gather.6.cloned.1.call-done), kind=kOutput, calls=%fused_computation.12 | convolution fusion | flops 4296015872 | bytes 10485760 | tf_op jit(solution)/shard_map/dot_general | solution.py:67
  280.6 1.3 copy-done
  281.9 1.8 convolution_bitcast_fusion
  283.7 0.2 multiply_reduce_fusion
  283.9 2.6 copy.19
  286.5 3.9 %copy.20 = bf16[1,1024,1024]{2,1,0:T(8,128)(2,1)} copy(bf16[1,1024,1024]{1,2,0:T(8,128)(2,1)} %bitcast.65) | data formatting | bytes 4194304
  290.4 0.7 multiply_convert_fusion
  (9 shorter events, 0.1 us)
Async XLA Ops:
  7.2 81.9 %all-gather.8.cloned.1.call-start = ((), (), s32[]{:S(2)}) async-start(), calls=%async_computation.1 | async-start | bytes 4456448 | tf_op jit(solution)/shard_map/all_gather | solution.py:56
  7.9 171.8 %all-gather.12.cloned.1.call-start = ((), (), s32[]{:S(2)}) async-start(), calls=%async_computation.3 | async-start | bytes 4456448 | tf_op jit(solution)/shard_map/all_gather | solution.py:55
  9.8 183.4 %all-gather.6.cloned.1.call-start = ((), (), s32[]{:S(2)}) async-start(), calls=%async_computation | async-start | bytes 6291456 | tf_op jit(solution)/shard_map/all_gather | solution.py:60
  10.5 262.1 %all-gather.10.cloned.1.call-start = ((), (), s32[]{:S(2)}) async-start(), calls=%async_computation.2 | async-start | bytes 4456448 | tf_op jit(solution)/shard_map/all_gather | solution.py:57
  202.4 81.3 %copy-start.1 = (f32[8]{0:T(128)S(1)}, f32[8]{0:T(128)}, u32[]{:S(2)}) copy-start(f32[8]{0:T(128)} %param.12) | copy-start | bytes 100
  280.6 1.3 copy-start
  283.9 6.5 %copy-start.2 = (f32[128]{0:T(128)S(1)}, f32[128]{0:T(128)}, u32[]{:S(2)}) copy-start(f32[128]{0:T(128)} %param.13) | copy-start | bytes 1540
Sparse Core Ops, SparseCore 0:
  10.7 78.3 all-gather.7
  92.4 87.3 all-gather.11
  181.3 11.8 all-gather.5
  195.8 76.7 all-gather.9
where the time goes:
time: 298 us
  waiting for transfers between devices  241 us (81%)
  matrix products  21.7 us (7%)
  local copies, waits for them, and re-layouts  16.1 us (5%)
  between operations  13.9 us (5%)
    all_gather x1, waiting for transfers between devices, body(): lax.all_gather(w_query, 'sp', axis=0, tiled=True)  84.1 us
    all_gather x1, waiting for transfers between devices, body(): lax.all_gather(w_key, 'sp', axis=0, tiled=True)  75.3 us
    all_gather x1, waiting for transfers between devices, body(): lax.all_gather(w_value, 'sp', axis=0, tiled=True)  70.2 us
    unnamed x9, local copies, waits for them, and re-layouts  9.62 us
    all_gather x1, waiting for transfers between devices, body(): lax.all_gather(prompt, 'tp', axis=2, tiled=True)  9.34 us
    dot_general x1, matrix products, body(): jnp.dot(row_piece, full_value, preferred_element_type=jnp.float32)  8.02 us
    dot_general x1, matrix products, body(): key_sum = jnp.dot(row_piece, full_key, preferred_element_type=jnp.float32)  7.59 us
    dot_general x1, local copies, waits for them, and re-layouts, body(): key_sum = jnp.dot(row_piece, full_key, preferred_element_type=jnp.float32)  6.5 us
  transfers between devices with their start and end apart: 4, of which 4 were waited for; matrix products, arithmetic and copies ran while one was open for 7% of the time, Pallas kernels for 0%

commit v1 on v0

--- a/solution.py
+++ b/solution.py
@@ -8,6 +8,14 @@
 LEN = 1024
 rope_base = 500000.0
 norm_eps = 1e-05
+
+
+def obtain_the_array(base_x, array_axis=0):
+    n_now = jnp.concatenate(
+        lax.all_to_all(jnp.stack([base_x for _ in range(lax.axis_size("sp"))]), "sp", 0, 0),
+        axis=array_axis,
+    )
+    return n_now
 
 
 def rotate(vectors, angle):
@@ -53,7 +61,7 @@
     inverse = inverse_freq()
     full_query, full_key, full_value = (
         lax.all_gather(w_query, "sp", axis=0, tiled=True),
-        lax.all_gather(w_key, "sp", axis=0, tiled=True),
+        obtain_the_array(w_key),
         lax.all_gather(w_value, "sp", axis=0, tiled=True),
     )
     pieces = (

time: 298 us -> 287 us (0.963)
  waiting for transfers between devices: 241 us -> 211 us
  local copies, waits for them, and re-layouts: 16.1 us -> 26.5 us
  starting transfers between devices: 0.16 us -> 8.65 us
    all_to_all x0 -> x1, waiting for transfers between devices: none -> 93.2 us  [obtain_the_array(): lax.all_to_all(jnp.stack([base_x for _ in range(lax.axis_size('sp'))]), '...]
    all_gather x1 -> x0, waiting for transfers between devices: 75.3 us -> none  [body(): lax.all_gather(w_key, 'sp', axis=0, tiled=True)]
    all_gather x1, waiting for transfers between devices: 84.1 us -> 35.4 us  [body(): lax.all_gather(w_query, 'sp', axis=0, tiled=True)]
    all_to_all x0 -> x1, starting transfers between devices: none -> 8.52 us  [obtain_the_array(): lax.all_to_all(jnp.stack([base_x for _ in range(lax.axis_size('sp'))]), '...]
    all_to_all x0 -> x1, local copies, waits for them, and re-layouts: none -> 6.45 us  [obtain_the_array(): lax.all_to_all(jnp.stack([base_x for _ in range(lax.axis_size('sp'))]), '...]
    unnamed x9 -> x12, local copies, waits for them, and re-layouts: 9.62 us -> 10.7 us
  transfers between devices with their start and end apart: 4 -> 4, of which waited for: 4 -> 4; matrix products, arithmetic and copies ran while one was open for 7% -> 11% of each run, Pallas kernels for 0% -> 0%
where the time goes in v1:
time: 287 us; the launch traced here: 286 us
  waiting for transfers between devices  211 us (74%)
  local copies, waits for them, and re-layouts  26.5 us (9%)
  matrix products  21.7 us (8%)
  between operations  13.9 us (5%)
  starting transfers between devices  8.65 us (3%)
    all_to_all x1, waiting for transfers between devices, obtain_the_array(): lax.all_to_all(jnp.stack([base_x for _ in range(lax.axis_size('sp'))]), '...  93.2 us
    all_gather x1, waiting for transfers between devices, body(): lax.all_gather(w_value, 'sp', axis=0, tiled=True)  70.3 us
    all_gather x1, waiting for transfers between devices, body(): lax.all_gather(w_query, 'sp', axis=0, tiled=True)  35.4 us
    all_gather x1, waiting for transfers between devices, body(): lax.all_gather(prompt, 'tp', axis=2, tiled=True)  10.9 us
    unnamed x12, local copies, waits for them, and re-layouts  10.7 us
    all_to_all x1, starting transfers between devices, obtain_the_array(): lax.all_to_all(jnp.stack([base_x for _ in range(lax.axis_size('sp'))]), '...  8.52 us
    dot_general x1, matrix products, body(): jnp.dot(row_piece, full_value, preferred_element_type=jnp.float32)  8.02 us
    dot_general x1, matrix products, body(): key_sum = jnp.dot(row_piece, full_key, preferred_element_type=jnp.float32)  7.59 us
  transfers between devices with their start and end apart: 4, of which 4 were waited for; matrix products, arithmetic and copies ran while one was open for 11% of the time, Pallas kernels for 0%

profile of v1, /device:TPU:0, one launch (start us, length us, event | category | flops | bytes accessed | tf_op | source)
XLA Modules:
  0.0 286.5 jit_solution(1684135463326081648)
XLA Ops:
  7.2 1.8 copy.30
  9.1 0.7 all-gather.5.cloned.1.call-update
  9.8 1.1 copy.27
  10.9 2.8 stack.2
  13.7 8.5 %all-to-all-start = ((bf16[16,128,1024]{1,2,0:T(8,128)(2,1)}), bf16[16,128,1024]{1,2,0:T(8,128)(2,1)}, u32[]{:S(2)}, u32[]{:S(2)}) async-start(bf16[16,128,1024]{1,2,0:T(8,128)(2,1)} %stack.2), calls=%async_computation | async-start | bytes 8388608 | tf_op jit(solution)/shard_map/all_to_all | solution.py:15
  22.2 0.0 all-gather.7.cloned.1.call-start
  22.3 0.7 all-gather.7.cloned.1.call-update
  23.0 1.8 all-gather
  24.8 0.1 multiply_sine_fusion
  24.8 0.5 fusion.15
  25.4 93.2 %all-to-all-done = bf16[16,128,1024]{1,2,0:T(8,128)(2,1)} async-done(((bf16[16,128,1024]{1,2,0:T(8,128)(2,1)}), bf16[16,128,1024]{1,2,0:T(8,128)(2,1)}, u32[]{:S(2)}, u32[]{:S(2)}) %all-to-all-start) | async-done | bytes 4194336 | tf_op jit(solution)/shard_map/all_to_all | solution.py:15
  118.6 6.5 %copy.28 = bf16[16,128,1024]{2,1,0:T(8,128)(2,1)} copy(bf16[16,128,1024]{1,2,0:T(8,128)(2,1)} %all-to-all-done) | data formatting | bytes 8388608 | tf_op jit(solution)/shard_map/all_to_all | solution.py:15
  125.0 6.5 %copy.29 = bf16[1024,2048]{1,0:T(8,128)(2,1)} copy(bf16[1024,2048]{0,1:T(8,128)(2,1)} %bitcast.60) | data formatting | bytes 8388608 | tf_op jit(solution)/shard_map/dot_general | solution.py:74
  131.6 35.4 %all-gather.9.cloned.1.call-done = bf16[2048,1024]{0,1:T(8,128)(2,1)} async-done(((bf16[128,1024]{0,1:T(8,128)(2,1)}), bf16[2048,1024]{0,1:T(8,128)(2,1)}) %all-gather.9.cloned.1.call-update) | async-done | bytes 4194320 | tf_op jit(solution)/shard_map/all_gather | solution.py:63
  166.9 3.9 %fusion.20 = f32[1,8,2,64]{3,0,2,1:T(1,128)S(1)} fusion(bf16[8,2,64,2048]{3,2,1,0:T(8,128)(2,1)} %bitcast.62, bf16[1,2048]{1,0:T(2,128)(2,1)S(1)} %all-gather), kind=kOutput, calls=%fused_computation.23 | convolution fusion | flops 4194304 | bytes 4202496 | tf_op jit(solution)/shard_map/dot_general | solution.py:76
  170.8 0.1 fusion.23
  170.9 0.1 maximum_bitcast_fusion
  171.0 10.9 %all-gather.5.cloned.1.call-done = bf16[1,1024,2048]{2,1,0:T(8,128)(2,1)} async-done(((bf16[1,1024,1024]{2,1,0:T(8,128)(2,1)}), bf16[1,1024,2048]{2,1,0:T(8,128)(2,1)}) %all-gather.5.cloned.1.call-update) | async-done | bytes 4194320 | tf_op jit(solution)/shard_map/all_gather | solution.py:68
  181.9 7.6 %fusion.4 = f32[1,1024,8,2,64]{1,4,3,2,0:T(8,128)S(1)} fusion(bf16[8,2,64,2048]{3,2,1,0:T(8,128)(2,1)} %bitcast.63, bf16[1,1024,2048]{2,1,0:T(8,128)(2,1)} %all-gather.5.cloned.1.call-done), kind=kOutput, calls=%fused_computation.4 | convolution fusion | flops 4294967296 | bytes 12582912 | tf_op jit(solution)/shard_map/dot_general | solution.py:74
  189.5 0.7 subtract_convert_fusion
  190.2 0.4 fusion.7
  190.6 0.1 fusion.25
  190.7 0.2 fusion.17
  190.9 0.2 pad_maximum_fusion
  191.1 70.3 %all-gather.7.cloned.1.call-done = bf16[2048,1024]{1,0:T(8,128)(2,1)} async-done(((bf16[128,1024]{1,0:T(8,128)(2,1)}), bf16[2048,1024]{1,0:T(8,128)(2,1)}) %all-gather.7.cloned.1.call-update) | async-done | bytes 4194320 | tf_op jit(solution)/shard_map/all_gather | solution.py:65
  261.4 8.0 %fusion.11 = bf16[1024,1024]{0,1:T(8,128)(2,1)S(1)} fusion(bf16[2048,1024]{1,0:T(8,128)(2,1)} %all-gather.7.cloned.1.call-done, bf16[1,1024,2048]{2,1,0:T(8,128)(2,1)} %all-gather.5.cloned.1.call-done), kind=kOutput, calls=%fused_computation.12 | convolution fusion | flops 4296015872 | bytes 10485760 | tf_op jit(solution)/shard_map/dot_general | solution.py:75
  269.5 1.3 copy-done
  270.8 1.8 convolution_bitcast_fusion
  272.6 0.2 multiply_reduce_fusion
  272.8 2.6 copy.33
  275.4 3.9 %copy.34 = bf16[1,1024,1024]{2,1,0:T(8,128)(2,1)} copy(bf16[1,1024,1024]{1,2,0:T(8,128)(2,1)} %bitcast.67) | data formatting | bytes 4194304
  279.3 0.7 multiply_convert_fusion
  (13 shorter events, 0.1 us)
Async XLA Ops:
  7.2 159.8 %all-gather.9.cloned.1.call-start = ((), (), s32[]{:S(2)}) async-start(), calls=%async_computation.3 | async-start | bytes 4456448 | tf_op jit(solution)/shard_map/all_gather | solution.py:63
  9.0 172.8 %all-gather.5.cloned.1.call-start = ((), (), s32[]{:S(2)}) async-start(), calls=%async_computation.1 | async-start | bytes 6291456 | tf_op jit(solution)/shard_map/all_gather | solution.py:68
  13.7 9.3 %copy-start.1 = (bf16[1,1024]{1,0:T(2,128)(2,1)S(1)}, bf16[1,1024]{1,0:T(2,128)(2,1)}, u32[]{:S(2)}) copy-start(bf16[1,1024]{1,0:T(2,128)(2,1)} %param.8) | copy-start | bytes 6148
  13.7 104.9 %all-to-all-start = ((bf16[16,128,1024]{1,2,0:T(8,128)(2,1)}), bf16[16,128,1024]{1,2,0:T(8,128)(2,1)}, u32[]{:S(2)}, u32[]{:S(2)}) async-start(bf16[16,128,1024]{1,2,0:T(8,128)(2,1)} %stack.2), calls=%async_computation | async-start | bytes 8388608 | tf_op jit(solution)/shard_map/all_to_all | solution.py:15
  22.2 239.2 %all-gather.7.cloned.1.call-start = ((), (), s32[]{:S(2)}) async-start(), calls=%async_computation.2 | async-start | bytes 4456448 | tf_op jit(solution)/shard_map/all_gather | solution.py:65
  191.1 81.5 %copy-start.2 = (f32[8]{0:T(128)S(1)}, f32[8]{0:T(128)}, u32[]{:S(2)}) copy-start(f32[8]{0:T(128)} %param.12) | copy-start | bytes 100
  269.5 1.3 copy-start
  272.8 6.5 %copy-start.3 = (f32[128]{0:T(128)S(1)}, f32[128]{0:T(128)}, u32[]{:S(2)}) copy-start(f32[128]{0:T(128)} %param.13) | copy-start | bytes 1540
Sparse Core Ops, SparseCore 0:
  11.2 155.6 all-gather.8
  168.5 13.3 all-gather.4
  184.6 76.7 all-gather.6
